TPU v7x, 32 devices: a whole 2x2x4 slice. The times are simulated.
32 devices in a mesh: sp: 8 (over z, y), tp: 4 (over x, core).
Axes of the slice: x: 2, y: 2, z: 4, core: 2. Of those that a mesh axis runs over, the one named last changes fastest.
Arguments:
- queries: bfloat16 [4096, 2048], P('sp', 'tp'), may hold values from -6 to 6
- keys: bfloat16 [4096, 512], P('sp', 'tp'), may hold values from -6 to 6
- values: bfloat16 [4096, 512], P('sp', 'tp'), may hold values from -6 to 6
- residual: bfloat16 [4096, 2048], P(('sp', 'tp')), may hold values from -0.119628906 to 0.119628906
- out_proj: bfloat16 [2048, 2048], replicated, may hold values from -0.125 to 0.125
- query_gain: float32 [128], replicated, may hold values from 0.7 to 7
- key_gain: float32 [128], replicated, may hold values from 0.7 to 7
- norm_gain: float32 [2048], replicated, may hold values from 0.1 to 1.9
- routes: int32 [4096, 4], P(('sp', 'tp')), may hold values from 0 to 31, all different within a row; in each aligned block of 128 rows (0 to 127, 128 to 255, ...) at most 32 rows name the same one
- route_weight: float32 [4096, 4], P(('sp', 'tp')), may hold values from 0.1 to 1
- expert_gate: bfloat16 [32, 2048, 256], P(('sp', 'tp')), may hold values from -0.125 to 0.125
- expert_up: bfloat16 [32, 2048, 256], P(('sp', 'tp')), may hold values from -0.125 to 0.125
- expert_down: bfloat16 [32, 256, 2048], P(('sp', 'tp')), may hold values from -0.375 to 0.375
- shared_gate: bfloat16 [2048, 256], replicated, may hold values from -0.125 to 0.125
- shared_up: bfloat16 [2048, 256], replicated, may hold values from -0.125 to 0.125
- shared_down: bfloat16 [256, 2048], replicated, may hold values from -0.375 to 0.375
Outputs:
- layer_out: bfloat16 [4096, 2048], P(('sp', 'tp'))
Inputs may be any that keep to these rules, and one draw needn't show every extreme that they name: In the rows of one device (aligned blocks of 128 tokens), no expert is named by more than 32 routes; some expert is named by exactly 32 routes of some device; the 4 experts of a token differ.
All inputs are finite; a program needn't handle non-finite values.
Results may differ from a plain program's by a relative error of at most 0.023.
The roundings to bfloat16 on the way count: a program that leaves them out, or rounds other values in their place, can miss the bound.
Values may be sent and summed in bfloat16 or wider, within the bound.
A program may use at most 128 MiB of HBM per device.

v0:
```python
import math
import jax
import jax.numpy as jnp
from jax import lax
from jax.sharding import PartitionSpec as P

HEADS = 16
KV_HEADS = 4
GRID_W = 64
EPS = 1e-06
THETA = 10000.0


def rotate_pairs(block, cosine, sine):
    first, second = jnp.split(block, 2, axis=-1)
    return jnp.concatenate(
        [first * cosine - second * sine, second * cosine + first * sine], axis=-1
    )


def normed_rotary(source, gain, heads, offset):
    count = source.shape[0]
    width = gain.shape[0]
    values_f = source.astype(jnp.float32).reshape(count, heads, width)
    values_f = (
        values_f * lax.rsqrt(jnp.mean(values_f * values_f, axis=-1, keepdims=True) + EPS) * gain
    )
    position = offset + jnp.arange(count, dtype=jnp.int32)
    grid_row = (position // GRID_W).astype(jnp.float32)
    grid_col = (position % GRID_W).astype(jnp.float32)
    quarter = width // 4
    inverse = jnp.power(THETA, -4.0 * jnp.arange(quarter, dtype=jnp.float32) / width)
    row_angle = (grid_row[:, None] * inverse[None, :])[:, None, :]
    col_angle = (grid_col[:, None] * inverse[None, :])[:, None, :]
    row_half, col_half = jnp.split(values_f, 2, axis=-1)
    turned = jnp.concatenate(
        [
            rotate_pairs(row_half, jnp.cos(row_angle), jnp.sin(row_angle)),
            rotate_pairs(col_half, jnp.cos(col_angle), jnp.sin(col_angle)),
        ],
        axis=-1,
    )
    return turned.reshape(count, heads * width).astype(jnp.bfloat16)


def expert_apply(arrived, expert_gate, expert_up, expert_down):
    sources, slots, width = arrived.shape
    local = expert_gate.shape[0]
    grouped = arrived.reshape(sources // local, local, slots, width)
    gate_part = jnp.einsum(
        "sech,ehf->secf", grouped, expert_gate, preferred_element_type=jnp.float32
    )
    up_part = jnp.einsum("sech,ehf->secf", grouped, expert_up, preferred_element_type=jnp.float32)
    hidden_e = (jax.nn.silu(gate_part) * up_part).astype(jnp.bfloat16)
    result = jnp.einsum("secf,efh->sech", hidden_e, expert_down, preferred_element_type=jnp.float32)
    return result.astype(jnp.bfloat16).reshape(sources, slots, width)


def body(
    queries,
    keys,
    values,
    residual,
    out_proj,
    query_gain,
    key_gain,
    norm_gain,
    routes,
    route_weight,
    expert_gate,
    expert_up,
    expert_down,
    shared_gate,
    shared_up,
    shared_down,
):
    tok_local = queries.shape[0]
    width = query_gain.shape[0]
    group = HEADS // KV_HEADS
    kv_local = keys.shape[1] // width
    scale = 1.0 / math.sqrt(width)
    offset = lax.axis_index("sp") * tok_local
    q_rot = normed_rotary(queries, query_gain, kv_local * group, offset)
    k_rot = normed_rotary(keys, key_gain, kv_local, offset)
    query_3d = q_rot.reshape(tok_local, kv_local, group, width).transpose(1, 2, 0, 3)
    query_3d = query_3d.reshape(kv_local, group * tok_local, width)
    start_state = (
        jnp.full((kv_local, group * tok_local), -jnp.inf, jnp.float32),
        jnp.zeros((kv_local, group * tok_local), jnp.float32),
        jnp.zeros((kv_local, group * tok_local, width), jnp.float32),
    )
    key_piece = lax.all_gather(k_rot, "sp", axis=0, tiled=True)
    value_piece = lax.all_gather(values, "sp", axis=0, tiled=True)
    count = key_piece.shape[0]
    block = math.gcd(count, 512)

    def one_block(index_block, state):
        running_max, running_sum, accum = state
        key_rows = lax.dynamic_slice_in_dim(key_piece, index_block * block, block, 0)
        value_rows = lax.dynamic_slice_in_dim(value_piece, index_block * block, block, 0)
        key_3d = key_rows.reshape(block, kv_local, width)
        value_3d = value_rows.reshape(block, kv_local, width)
        scores = (
            jnp.einsum("gqd,kgd->gqk", query_3d, key_3d, preferred_element_type=jnp.float32) * scale
        )
        new_max = jnp.maximum(running_max, jnp.max(scores, axis=-1))
        weights = jnp.exp(scores - new_max[..., None])
        factor = jnp.exp(running_max - new_max)
        new_sum = running_sum * factor + jnp.sum(weights, axis=-1)
        added = jnp.einsum(
            "gqk,kgd->gqd",
            weights.astype(jnp.bfloat16),
            value_3d,
            preferred_element_type=jnp.float32,
        )
        return (new_max, new_sum, accum * factor[..., None] + added)

    final_max, final_sum, final_acc = lax.fori_loop(0, count // block, one_block, start_state)
    attn_local = (final_acc / final_sum[..., None]).astype(jnp.bfloat16)
    attn_local = attn_local.reshape(kv_local, group, tok_local, width).transpose(2, 0, 1, 3)
    attn_local = attn_local.reshape(tok_local, kv_local * group * width)
    all_heads = lax.all_to_all(attn_local, "tp", split_axis=0, concat_axis=1, tiled=True)
    projected = jnp.dot(all_heads, out_proj, preferred_element_type=jnp.float32)
    hidden1 = (residual.astype(jnp.float32) + projected).astype(jnp.bfloat16)
    hidden_f = hidden1.astype(jnp.float32)
    normed = (
        hidden_f
        * lax.rsqrt(jnp.mean(hidden_f * hidden_f, axis=-1, keepdims=True) + EPS)
        * norm_gain
    ).astype(jnp.bfloat16)
    rows_local = normed.shape[0]
    top_count = routes.shape[1]
    pair_count = rows_local * top_count
    expert_total = expert_gate.shape[0] * lax.axis_size("sp") * lax.axis_size("tp")
    capacity = max(2, 2 * rows_local * top_count // expert_total)
    flat_routes = routes.reshape(pair_count)
    one_hot = (flat_routes[:, None] == jnp.arange(expert_total, dtype=jnp.int32)[None, :]).astype(
        jnp.float32
    )
    lower = (jnp.arange(pair_count)[:, None] >= jnp.arange(pair_count)[None, :]).astype(jnp.float32)
    running_count = jnp.dot(lower, one_hot, precision=lax.Precision.HIGHEST)
    slot_place = (jnp.sum(running_count * one_hot, axis=1) - 1.0).astype(jnp.int32)
    slot_index = flat_routes * capacity + slot_place
    slot_total = expert_total * capacity
    placement = (jnp.arange(slot_total, dtype=jnp.int32)[:, None] == slot_index[None, :]).astype(
        jnp.bfloat16
    )
    placement = jnp.sum(placement.reshape(slot_total, rows_local, top_count), axis=2)
    send_rows = jnp.dot(placement, normed, preferred_element_type=jnp.float32).astype(jnp.bfloat16)
    send_rows = send_rows.reshape(expert_total, capacity, normed.shape[1])
    shared_hidden = (
        jax.nn.silu(jnp.dot(normed, shared_gate, preferred_element_type=jnp.float32))
        * jnp.dot(normed, shared_up, preferred_element_type=jnp.float32)
    ).astype(jnp.bfloat16)
    shared_out = jnp.dot(shared_hidden, shared_down, preferred_element_type=jnp.float32)
    processed = expert_apply(
        lax.all_to_all(send_rows, ("sp", "tp"), split_axis=0, concat_axis=0, tiled=True),
        expert_gate,
        expert_up,
        expert_down,
    )
    returned = lax.all_to_all(processed, ("sp", "tp"), split_axis=0, concat_axis=0, tiled=True)
    returned = returned.reshape(slot_total, normed.shape[1])
    routed = (
        returned[slot_index].reshape(rows_local, top_count, normed.shape[1]).astype(jnp.float32)
    )
    mixed = jnp.einsum("tk,tkd->td", route_weight, routed) + shared_out
    return (hidden_f + mixed).astype(jnp.bfloat16)


def solution(mesh):
    placed = (
        P("sp", "tp"),
        P("sp", "tp"),
        P("sp", "tp"),
        P(("sp", "tp"), None),
        P(),
        P(),
        P(),
        P(),
        P(("sp", "tp"), None),
        P(("sp", "tp"), None),
        P(("sp", "tp"), None, None),
        P(("sp", "tp"), None, None),
        P(("sp", "tp"), None, None),
        P(),
        P(),
        P(),
    )
    return jax.shard_map(
        body, mesh=mesh, in_specs=placed, out_specs=P(("sp", "tp"), None), check_vma=False
    )
```

profile of v0, /device:TPU:0, one launch (start us, length us, event | category | flops | bytes accessed | tf_op | source)
XLA Modules:
  0.0 420.8 jit_solution(3090994777994951920)
XLA Ops:
  19.2 32.9 %all-gather.6.cloned.1.call-done = bf16[4096,1,128]{0,2,1:T(8,128)(2,1)} async-done(((bf16[512,1,128]{0,2,1:T(8,128)(2,1)}), bf16[4096,1,128]{0,2,1:T(8,128)(2,1)}) %all-gather.6.cloned.1.call-update) | async-done | bytes 1048592 | tf_op jit(solution)/shard_map/all_gather | solution.py:92
  52.1 41.4 %all-gather.4.cloned.1.call-done = bf16[4096,128]{1,0:T(8,128)(2,1)} async-done(((bf16[512,128]{1,0:T(8,128)(2,1)}), bf16[4096,128]{1,0:T(8,128)(2,1)}) %all-gather.4.cloned.1.call-update) | async-done | bytes 1048592 | tf_op jit(solution)/shard_map/all_gather | solution.py:93
  93.6 73.7 %while.18 = (s32[]{:T(128)}, f32[1,2048]{1,0:T(1,128)S(1)}, f32[1,2048]{1,0:T(1,128)S(1)}, f32[1,2048,128]{2,1,0:T(8,128)S(1)}, bf16[4096,128]{0,1:T(8,128)(2,1)...) while((s32[]{:T(128)}, f32[1,2048]{1,0:T(1,128)S(1)}, ...), condition=%wide.region_5.6_spmd.clone, body=%wide.region_2.5_spmd.clone.sunk | while | flops 546056192 | bytes 32374984 | solution.py:118
  93.6 3.6 multiply_reduce_fusion.4
  97.2 3.0 fusion.96
  102.8 3.6 multiply_reduce_fusion.4
  106.4 3.0 fusion.96
  112.0 3.6 multiply_reduce_fusion.4
  115.6 3.0 fusion.96
  119.0 2.1 fusion.98
  121.2 3.6 multiply_reduce_fusion.4
  124.8 3.0 fusion.96
  130.4 3.6 multiply_reduce_fusion.4
  134.1 3.0 fusion.96
  139.7 3.6 multiply_reduce_fusion.4
  143.3 3.0 fusion.96
  148.9 3.6 multiply_reduce_fusion.4
  152.5 3.0 fusion.96
  158.1 3.6 multiply_reduce_fusion.4
  161.7 3.0 fusion.96
  169.1 3.7 all-to-all-start
  173.2 8.1 %all-to-all-done = bf16[4,128,512]{2,1,0:T(8,128)(2,1)S(1)} async-done(((bf16[4,128,512]{2,1,0:T(8,128)(2,1)}), bf16[4,128,512]{2,1,0:T(8,128)(2,1)S(1)}, u32[]{:S(2)}, u32[]{:S(2)}) %all-to-all-start) | async-done | bytes 524320 | tf_op jit(solution)/shard_map/all_to_all | solution.py:122
  181.6 4.7 %multiply_reduce_fusion.1 = (f32[128]{0:T(128)S(1)}, f32[128,2048]{1,0:T(8,128)S(1)}) fusion(bf16[128,2048]{0,1:T(8,128)(2,1)S(1)} %bitcast.106, bf16[2048,2048]{1,0:T(8,128)(2,1)} %param.22, bf16[128,2048]{1,0:T(8,128)(2,1)S(1)} %copy-done.5), kind=kOutput, calls=%fused_computation.52 | convolution fusion | flops 1075314560 | bytes 10486272 | tf_op jit(solution)/shard_map/dot_general | solution.py:123
  187.8 95.8 %all_to_all.29 = bf16[32,32,2048]{2,1,0:T(8,128)(2,1)S(1)} all-to-all(bf16[32,32,2048]{2,1,0:T(8,128)(2,1)S(1)} %bitcast.103), channel_id=1, replica_groups=mesh['sp'=8,'tp'=4] {'sp','tp'}, dimensions={0} | all-to-all | bytes 8388608 | tf_op jit(solution)/shard_map/all_to_all | solution.py:157
  285.6 2.3 convolution_bitcast_fusion.2
  287.9 9.1 %convolution_convert_fusion = bf16[32,32,2048]{2,1,0:T(8,128)(2,1)} fusion(bf16[32,32,2048]{2,1,0:T(8,128)(2,1)} %copy-done.2, bf16[1,256,2048]{2,1,0:T(8,128)(2,1)S(1)} %copy-done, bf16[1,2048,256]{2,1,0:T(8,128)(2,1)} %param.29, f32[32,1,32,256]{3,2,0,1:T(8,128)} %convolution_bitcast_fusion.2), kind=kOutput, calls=%fused_computation.23 | convolution fusion | flops 2151153664 | bytes 11534336 | tf_op jit(solution)/shard_map/secf,efh->sech/dot_general | solution.py:55
  297.0 4.0 all-to-all-start.2
  301.7 93.0 %all-to-all-done.2 = bf16[32,32,2048]{2,1,0:T(8,128)(2,1)} async-done(((bf16[32,32,2048]{2,1,0:T(8,128)(2,1)}), bf16[32,32,2048]{2,1,0:T(8,128)(2,1)}, u32[]{:S(2)}, u32[]{:S(2)}) %all-to-all-start.2) | async-done | bytes 4194336 | tf_op jit(solution)/shard_map/all_to_all | solution.py:162
  394.7 8.0 %gather_fusion = bf16[512,2048]{1,0:T(8,128)(2,1)} fusion(bf16[1024,2048]{1,0:T(8,128)(2,1)} %bitcast.29, s32[1024]{0:T(1024)S(1)} %pad_clamp_fusion), kind=kCustom, calls=%fused_computation | custom fusion | bytes 4196352 | tf_op jit(solution)/shard_map/gather | solution.py:165
  402.7 4.2 reshape.478
  406.9 3.8 fusion.76
  410.7 3.3 fusion.19
  (109 shorter events, 37.1 us)
Async XLA Ops:
  6.5 281.3 %copy-start = (bf16[1,256,2048]{2,1,0:T(8,128)(2,1)S(1)}, bf16[1,256,2048]{2,1,0:T(8,128)(2,1)}, u32[]{:S(2)}) copy-start(bf16[1,256,2048]{2,1,0:T(8,128)(2,1)} %param.30) | copy-start | bytes 3145732
  6.5 7.9 %copy-start.9 = (f32[128]{0:T(128)S(1)}, f32[128]{0:T(128)}, u32[]{:S(2)}) copy-start(f32[128]{0:T(128)} %param.23) | copy-start | bytes 1540
  6.5 45.6 %all-gather.6.cloned.1.call-start = ((), (), s32[]{:S(2)}) async-start(), calls=%async_computation.4 | async-start | bytes 1179648 | tf_op jit(solution)/shard_map/all_gather | solution.py:92
  9.7 83.8 %all-gather.4.cloned.1.call-start = ((), (), s32[]{:S(2)}) async-start(), calls=%async_computation.3 | async-start | bytes 1179648 | tf_op jit(solution)/shard_map/all_gather | solution.py:93
  15.2 3.5 copy-start.7
  97.2 3.4 copy-start.1
  106.4 3.4 copy-start.1
  115.6 3.4 copy-start.1
  124.8 3.4 copy-start.1
  134.0 3.4 copy-start.1
  143.3 3.4 copy-start.1
  152.5 3.4 copy-start.1
  161.7 3.4 copy-start.1
  167.3 14.3 %copy-start.5 = (bf16[128,2048]{1,0:T(8,128)(2,1)S(1)}, bf16[128,2048]{1,0:T(8,128)(2,1)}, u32[]{:S(2)}) copy-start(bf16[128,2048]{1,0:T(8,128)(2,1)} %param.21) | copy-start | bytes 1572868
  169.1 12.3 %all-to-all-start = ((bf16[4,128,512]{2,1,0:T(8,128)(2,1)}), bf16[4,128,512]{2,1,0:T(8,128)(2,1)S(1)}, u32[]{:S(2)}, u32[]{:S(2)}) async-start(bf16[4,128,512]{2,1,0:T(8,128)(2,1)} %all_to_all.20), calls=%async_computation | async-start | bytes 1048576 | tf_op jit(solution)/shard_map/all_to_all | solution.py:122
  181.6 4.8 %copy-start.6 = (f32[2048]{0:T(1024)S(1)}, f32[2048]{0:T(1024)}, u32[]{:S(2)}) copy-start(f32[2048]{0:T(1024)} %param.25) | copy-start | bytes 24580
  187.7 97.8 %copy-start.10 = (bf16[1,2048,256]{2,1,0:T(8,128)(2,1)S(1)}, bf16[1,2048,256]{2,1,0:T(8,128)(2,1)}, u32[]{:S(2)}) copy-start(bf16[1,2048,256]{2,1,0:T(8,128)(2,1)} %param.28) | copy-start | bytes 3145732
  283.6 2.0 copy-start.2
  297.0 4.1 copy-start.8
  297.0 4.3 %copy-start.4 = (bf16[2048,256]{1,0:T(8,128)(2,1)S(1)}, bf16[2048,256]{1,0:T(8,128)(2,1)}, u32[]{:S(2)}) copy-start(bf16[2048,256]{1,0:T(8,128)(2,1)} %param.31) | copy-start | bytes 3145732
  297.0 97.7 %all-to-all-start.2 = ((bf16[32,32,2048]{2,1,0:T(8,128)(2,1)}), bf16[32,32,2048]{2,1,0:T(8,128)(2,1)}, u32[]{:S(2)}, u32[]{:S(2)}) async-start(bf16[32,32,2048]{2,1,0:T(8,128)(2,1)} %convolution_convert_fusion), calls=%async_computation.2 | async-start | bytes 8388608 | tf_op jit(solution)/shard_map/all_to_all | solution.py:162
  402.7 8.0 %copy-start.3 = (bf16[256,2048]{1,0:T(8,128)(2,1)S(1)}, bf16[256,2048]{1,0:T(8,128)(2,1)}, u32[]{:S(2)}) copy-start(bf16[256,2048]{1,0:T(8,128)(2,1)} %param.33) | copy-start | bytes 3145732
Sparse Core Ops, SparseCore 0:
  9.9 42.2 all-gather.5
  54.2 39.2 all-gather.3
where the time goes:
time: 422 us; the launch traced here: 421 us
  waiting for transfers between devices  176 us (42%)
  blocking collectives  95.8 us (23%)
  matrix products  71 us (17%)
  other arithmetic  34.1 us (8%)
  local copies, waits for them, and re-layouts  21.8 us (5%)
  between operations  13.7 us (3%)
  starting transfers between devices  7.71 us (2%)
    all_to_all x1, blocking collectives, body(): lax.all_to_all(send_rows, ('sp', 'tp'), split_axis=0, concat_axis=0, tile...  95.8 us
    all_to_all x1, waiting for transfers between devices, body(): lax.all_to_all(processed, ('sp', 'tp'), split_axis=0, concat_axis=0, tile...  93 us
    all_gather x1, waiting for transfers between devices, body(): value_piece = lax.all_gather(values, 'sp', axis=0, tiled=True)  41.4 us
    all_gather x1, waiting for transfers between devices, body(): key_piece = lax.all_gather(k_rot, 'sp', axis=0, tiled=True)  32.9 us
    dot_general x8, matrix products, one_block(): jnp.einsum('gqd,kgd->gqk', query_3d, key_3d, preferred_element_type=jnp.f...  28.8 us
    reduce_sum x8, other arithmetic, one_block(): new_sum = running_sum * factor + jnp.sum(weights, axis=-1)  24.4 us
    dot_general x8, matrix products, one_block(): jnp.einsum('gqk,kgd->gqd', weights.astype(jnp.bfloat16), value_3d, prefer...  17.1 us
    dot_general x1, matrix products, expert_apply(): jnp.einsum('secf,efh->sech', hidden_e, expert_down, preferred_element_typ...  9.08 us
  transfers between devices with their start and end apart: 4, of which 4 were waited for; matrix products, arithmetic and copies ran while one was open for 2% of the time, Pallas kernels for 0%

commit v1 on v0

--- a/solution.py
+++ b/solution.py
@@ -90,7 +90,12 @@
         jnp.zeros((kv_local, group * tok_local, width), jnp.float32),
     )
     key_piece = lax.all_gather(k_rot, "sp", axis=0, tiled=True)
-    value_piece = lax.all_gather(values, "sp", axis=0, tiled=True)
+    ring = [values]
+    for hop in range(7):
+        ring.append(lax.ppermute(ring[-1], "sp", [(dev, (dev + 1) % 8) for dev in range(8)]))
+    value_piece = jnp.roll(
+        jnp.concatenate(ring[::-1], axis=0), (lax.axis_index("sp") + 1) * ring[0].shape[0], axis=0
+    )
     count = key_piece.shape[0]
     block = math.gcd(count, 512)
 

time: 422 us -> 403 us (0.955)
  waiting for transfers between devices: 176 us -> 145 us
  local copies, waits for them, and re-layouts: 21.8 us -> 31 us
    ppermute x0 -> x7, waiting for transfers between devices: none -> 43.7 us  [body(): lax.ppermute(ring[-1], 'sp', [(dev, (dev + 1) % 8) for dev in range(8)])]
    all_gather x1 -> x0, waiting for transfers between devices: 41.4 us -> none  [body(): value_piece = lax.all_gather(values, 'sp', axis=0, tiled=True)]
    all_gather x1, waiting for transfers between devices: 32.9 us -> 0.01 us  [body(): key_piece = lax.all_gather(k_rot, 'sp', axis=0, tiled=True)]
    unnamed x23 -> x50, local copies, waits for them, and re-layouts: 3.38 us -> 11.6 us
  transfers between devices with their start and end apart: 4 -> 10, of which waited for: 4 -> 9; matrix products, arithmetic and copies ran while one was open for 2% -> 6% of each run, Pallas kernels for 0% -> 0%
where the time goes in v1:
time: 403 us; the launch traced here: 402 us
  waiting for transfers between devices  145 us (36%)
  blocking collectives  95.5 us (24%)
  matrix products  71.7 us (18%)
  other arithmetic  34.1 us (8%)
  local copies, waits for them, and re-layouts  31 us (8%)
  between operations  13.9 us (3%)
  starting transfers between devices  10.2 us (3%)
    all_to_all x1, blocking collectives, body(): lax.all_to_all(send_rows, ('sp', 'tp'), split_axis=0, concat_axis=0, tile...  95.5 us
    all_to_all x1, waiting for transfers between devices, body(): lax.all_to_all(processed, ('sp', 'tp'), split_axis=0, concat_axis=0, tile...  93 us
    ppermute x7, waiting for transfers between devices, body(): lax.ppermute(ring[-1], 'sp', [(dev, (dev + 1) % 8) for dev in range(8)])  43.7 us
    dot_general x8, matrix products, one_block(): jnp.einsum('gqd,kgd->gqk', query_3d, key_3d, preferred_element_type=jnp.f...  28.8 us
    reduce_sum x8, other arithmetic, one_block(): new_sum = running_sum * factor + jnp.sum(weights, axis=-1)  24.4 us
    dot_general x8, matrix products, one_block(): jnp.einsum('gqk,kgd->gqd', weights.astype(jnp.bfloat16), value_3d, prefer...  17.1 us
    unnamed x50, local copies, waits for them, and re-layouts  11.6 us
    dot_general x1, matrix products, expert_apply(): jnp.einsum('secf,efh->sech', hidden_e, expert_down, preferred_element_typ...  9.08 us
  transfers between devices with their start and end apart: 10, of which 9 were waited for; matrix products, arithmetic and copies ran while one was open for 6% of the time, Pallas kernels for 0%

profile of v1, /device:TPU:0, one launch (start us, length us, event | category | flops | bytes accessed | tf_op | source)
XLA Modules:
  0.0 401.8 jit_solution(1445348401114704467)
XLA Ops:
  16.9 7.1 %collective-permute-done.1 = bf16[512,128]{1,0:T(8,128)(2,1)S(1)} collective-permute-done((bf16[512,128]{1,0:T(8,128)(2,1)S(1)}, bf16[512,128]{1,0:T(8,128)(2,1)S(1)}, u32[]{:S(2)}, u32[]{:S(2)}) %collective-permute-start.1) | collective-permute-done | bytes 131104 | tf_op jit(solution)/shard_map/ppermute | solution.py:95
  24.0 9.0 %collective-permute-done.2 = bf16[512,128]{1,0:T(8,128)(2,1)S(1)} collective-permute-done((bf16[512,128]{1,0:T(8,128)(2,1)S(1)}, bf16[512,128]{1,0:T(8,128)(2,1)S(1)}, u32[]{:S(2)}, u32[]{:S(2)}) %collective-permute-start.2) | collective-permute-done | bytes 131104 | tf_op jit(solution)/shard_map/ppermute | solution.py:95
  33.8 6.9 %collective-permute-done.3 = bf16[512,128]{1,0:T(8,128)(2,1)S(1)} collective-permute-done((bf16[512,128]{1,0:T(8,128)(2,1)S(1)}, bf16[512,128]{1,0:T(8,128)(2,1)S(1)}, u32[]{:S(2)}, u32[]{:S(2)}) %collective-permute-start.3) | collective-permute-done | bytes 131104 | tf_op jit(solution)/shard_map/ppermute | solution.py:95
  42.6 7.8 %collective-permute-done.4 = bf16[512,128]{1,0:T(8,128)(2,1)S(1)} collective-permute-done((bf16[512,128]{1,0:T(8,128)(2,1)S(1)}, bf16[512,128]{1,0:T(8,128)(2,1)S(1)}, u32[]{:S(2)}, u32[]{:S(2)}) %collective-permute-start.4) | collective-permute-done | bytes 131104 | tf_op jit(solution)/shard_map/ppermute | solution.py:95
  52.2 6.2 %collective-permute-done.5 = bf16[512,128]{1,0:T(8,128)(2,1)} collective-permute-done((bf16[512,128]{1,0:T(8,128)(2,1)S(1)}, bf16[512,128]{1,0:T(8,128)(2,1)}, u32[]{:S(2)}, u32[]{:S(2)}) %collective-permute-start.5) | collective-permute-done | bytes 131104 | tf_op jit(solution)/shard_map/ppermute | solution.py:95
  62.0 4.4 %collective-permute-done.6 = bf16[512,128]{1,0:T(8,128)(2,1)} collective-permute-done((bf16[512,128]{1,0:T(8,128)(2,1)}, bf16[512,128]{1,0:T(8,128)(2,1)}, u32[]{:S(2)}, u32[]{:S(2)}) %collective-permute-start.6) | collective-permute-done | bytes 131104 | tf_op jit(solution)/shard_map/ppermute | solution.py:95
  75.1 73.8 %while.18 = (s32[]{:T(128)}, f32[1,2048]{1,0:T(1,128)S(1)}, f32[1,2048]{1,0:T(1,128)S(1)}, f32[1,2048,128]{2,1,0:T(8,128)S(1)}, bf16[4096,128]{0,1:T(8,128)(2,1)...) while((s32[]{:T(128)}, f32[1,2048]{1,0:T(1,128)S(1)}, ...), condition=%wide.region_5.6_spmd.clone, body=%wide.region_2.5_spmd.clone.sunk | while | flops 546056192 | bytes 32374992 | solution.py:123
  75.1 3.6 multiply_reduce_fusion.4
  78.7 3.0 fusion.96
  84.3 3.6 multiply_reduce_fusion.4
  88.0 3.0 fusion.96
  93.6 3.6 multiply_reduce_fusion.4
  97.2 3.0 fusion.96
  102.8 3.6 multiply_reduce_fusion.4
  106.4 3.0 fusion.96
  112.0 3.6 multiply_reduce_fusion.4
  121.3 3.6 multiply_reduce_fusion.4
  124.9 3.0 fusion.96
  130.5 3.6 multiply_reduce_fusion.4
  134.1 3.0 fusion.96
  139.7 3.6 multiply_reduce_fusion.4
  150.7 3.5 all-to-all-start
  154.7 8.3 %all-to-all-done = bf16[4,128,512]{2,1,0:T(8,128)(2,1)S(1)} async-done(((bf16[4,128,512]{2,1,0:T(8,128)(2,1)}), bf16[4,128,512]{2,1,0:T(8,128)(2,1)S(1)}, u32[]{:S(2)}, u32[]{:S(2)}) %all-to-all-start) | async-done | bytes 524320 | tf_op jit(solution)/shard_map/all_to_all | solution.py:127
  163.3 4.7 %multiply_reduce_fusion.1 = (f32[128]{0:T(128)S(1)}, f32[128,2048]{1,0:T(8,128)S(1)}) fusion(bf16[128,2048]{0,1:T(8,128)(2,1)S(1)} %bitcast.106, bf16[2048,2048]{1,0:T(8,128)(2,1)} %param.22, bf16[128,2048]{1,0:T(8,128)(2,1)S(1)} %copy-done.5), kind=kOutput, calls=%fused_computation.52 | convolution fusion | flops 1075314560 | bytes 10486272 | tf_op jit(solution)/shard_map/dot_general | solution.py:128
  169.4 95.5 %all_to_all.29 = bf16[32,32,2048]{2,1,0:T(8,128)(2,1)S(1)} all-to-all(bf16[32,32,2048]{2,1,0:T(8,128)(2,1)S(1)} %bitcast.103), channel_id=1, replica_groups=mesh['sp'=8,'tp'=4] {'sp','tp'}, dimensions={0} | all-to-all | bytes 8388608 | tf_op jit(solution)/shard_map/all_to_all | solution.py:162
  269.2 9.1 %convolution_convert_fusion = bf16[32,32,2048]{2,1,0:T(8,128)(2,1)} fusion(bf16[32,32,2048]{2,1,0:T(8,128)(2,1)} %copy-done.2, bf16[1,256,2048]{2,1,0:T(8,128)(2,1)S(1)} %copy-done, bf16[1,2048,256]{2,1,0:T(8,128)(2,1)} %param.29, f32[32,1,32,256]{3,2,0,1:T(8,128)} %convolution_bitcast_fusion.2), kind=kOutput, calls=%fused_computation.23 | convolution fusion | flops 2151153664 | bytes 11534336 | tf_op jit(solution)/shard_map/secf,efh->sech/dot_general | solution.py:55
  278.3 3.7 all-to-all-start.2
  282.7 93.0 %all-to-all-done.2 = bf16[32,32,2048]{2,1,0:T(8,128)(2,1)} async-done(((bf16[32,32,2048]{2,1,0:T(8,128)(2,1)}), bf16[32,32,2048]{2,1,0:T(8,128)(2,1)}, u32[]{:S(2)}, u32[]{:S(2)}) %all-to-all-start.2) | async-done | bytes 4194336 | tf_op jit(solution)/shard_map/all_to_all | solution.py:167
  375.7 8.0 %gather_fusion = bf16[512,2048]{1,0:T(8,128)(2,1)} fusion(bf16[1024,2048]{1,0:T(8,128)(2,1)} %bitcast.29, s32[1024]{0:T(1024)S(1)} %pad_clamp_fusion), kind=kCustom, calls=%fused_computation | custom fusion | bytes 4196352 | tf_op jit(solution)/shard_map/gather | solution.py:170
  383.7 4.1 %reshape.478 = bf16[128,4,2048]{2,1,0:T(4,128)(2,1)} reshape(bf16[512,2048]{1,0:T(8,128)(2,1)} %gather_fusion) | data formatting | bytes 4194304 | tf_op jit(solution)/shard_map/reshape | solution.py:170
  387.8 3.9 fusion.76
  391.7 3.3 fusion.19
  (149 shorter events, 62.0 us)
Async XLA Ops:
  6.5 262.7 %copy-start = (bf16[1,256,2048]{2,1,0:T(8,128)(2,1)S(1)}, bf16[1,256,2048]{2,1,0:T(8,128)(2,1)}, u32[]{:S(2)}) copy-start(bf16[1,256,2048]{2,1,0:T(8,128)(2,1)} %param.30) | copy-start | bytes 3145732
  6.5 68.6 %all-gather.3.cloned.1.call-start = ((), (), s32[]{:S(2)}) async-start(), calls=%async_computation.3 | async-start | bytes 1179648 | tf_op jit(solution)/shard_map/all_gather | solution.py:92
  6.5 9.7 %collective-permute-start = (bf16[512,128]{1,0:T(8,128)(2,1)}, bf16[512,128]{1,0:T(8,128)(2,1)S(1)}, u32[]{:S(2)}, u32[]{:S(2)}) collective-permute-start(bf16[512,128]{1,0:T(8,128)(2,1)} %param.20), channel_id=1, source_target_pairs={{0,4},{4,8},{8,12},{12,16},{16,20},{20,24},{24,28},{28,0},{1,5},{5... | collective-permute-start | bytes 393224 | tf_op jit(solution)/shard_map/ppermute | solution.py:95
  11.4 21.6 %copy-start.15 = (f32[128]{0:T(128)S(1)}, f32[128]{0:T(128)}, u32[]{:S(2)}) copy-start(f32[128]{0:T(128)} %param.23) | copy-start | bytes 1540
  16.3 7.7 %collective-permute-start.1 = (bf16[512,128]{1,0:T(8,128)(2,1)S(1)}, bf16[512,128]{1,0:T(8,128)(2,1)S(1)}, u32[]{:S(2)}, u32[]{:S(2)}) collective-permute-start(bf16[512,128]{1,0:T(8,128)(2,1)S(1)} %collective-permute-done), channel_id=1, source_target_pairs={{0,4},{4,8},{8,12},{12,16},{16,20},{20,24},{24,28},{28,0},{1,5},{5... | collective-permute-start | bytes 393224 | tf_op jit(solution)/shard_map/ppermute | solution.py:95
  24.0 9.1 %collective-permute-start.2 = (bf16[512,128]{1,0:T(8,128)(2,1)S(1)}, bf16[512,128]{1,0:T(8,128)(2,1)S(1)}, u32[]{:S(2)}, u32[]{:S(2)}) collective-permute-start(bf16[512,128]{1,0:T(8,128)(2,1)S(1)} %collective-permute-done.1), channel_id=1, source_target_pairs={{0,4},{4,8},{8,12},{12,16},{16,20},{20,24},{24,28},{28,0},{1,5},{5... | collective-permute-start | bytes 393224 | tf_op jit(solution)/shard_map/ppermute | solution.py:95
  33.0 19.2 %copy-start.7 = (bf16[512,128]{1,0:T(8,128)(2,1)}, bf16[512,128]{1,0:T(8,128)(2,1)S(1)}, u32[]{:S(2)}) copy-start(bf16[512,128]{1,0:T(8,128)(2,1)S(1)} %collective-permute-done.2) | copy-start | bytes 393220
  33.0 7.7 %collective-permute-start.3 = (bf16[512,128]{1,0:T(8,128)(2,1)S(1)}, bf16[512,128]{1,0:T(8,128)(2,1)S(1)}, u32[]{:S(2)}, u32[]{:S(2)}) collective-permute-start(bf16[512,128]{1,0:T(8,128)(2,1)S(1)} %collective-permute-done.2), channel_id=1, source_target_pairs={{0,4},{4,8},{8,12},{12,16},{16,20},{20,24},{24,28},{28,0},{1,5},{5... | collective-permute-start | bytes 393224 | tf_op jit(solution)/shard_map/ppermute | solution.py:95
  40.7 11.5 %copy-start.9 = (bf16[512,128]{1,0:T(8,128)(2,1)}, bf16[512,128]{1,0:T(8,128)(2,1)S(1)}, u32[]{:S(2)}) copy-start(bf16[512,128]{1,0:T(8,128)(2,1)S(1)} %collective-permute-done.3) | copy-start | bytes 393220
  40.7 9.7 %collective-permute-start.4 = (bf16[512,128]{1,0:T(8,128)(2,1)S(1)}, bf16[512,128]{1,0:T(8,128)(2,1)S(1)}, u32[]{:S(2)}, u32[]{:S(2)}) collective-permute-start(bf16[512,128]{1,0:T(8,128)(2,1)S(1)} %collective-permute-done.3), channel_id=1, source_target_pairs={{0,4},{4,8},{8,12},{12,16},{16,20},{20,24},{24,28},{28,0},{1,5},{5... | collective-permute-start | bytes 393224 | tf_op jit(solution)/shard_map/ppermute | solution.py:95
  50.4 8.0 %collective-permute-start.5 = (bf16[512,128]{1,0:T(8,128)(2,1)S(1)}, bf16[512,128]{1,0:T(8,128)(2,1)}, u32[]{:S(2)}, u32[]{:S(2)}) collective-permute-start(bf16[512,128]{1,0:T(8,128)(2,1)S(1)} %collective-permute-done.4), channel_id=1, source_target_pairs={{0,4},{4,8},{8,12},{12,16},{16,20},{20,24},{24,28},{28,0},{1,5},{5... | collective-permute-start | bytes 393224 | tf_op jit(solution)/shard_map/ppermute | solution.py:95
  58.4 8.0 %collective-permute-start.6 = (bf16[512,128]{1,0:T(8,128)(2,1)}, bf16[512,128]{1,0:T(8,128)(2,1)}, u32[]{:S(2)}, u32[]{:S(2)}) collective-permute-start(bf16[512,128]{1,0:T(8,128)(2,1)} %collective-permute-done.5), channel_id=1, source_target_pairs={{0,4},{4,8},{8,12},{12,16},{16,20},{20,24},{24,28},{28,0},{1,5},{5... | collective-permute-start | bytes 393224 | tf_op jit(solution)/shard_map/ppermute | solution.py:95
  60.0 11.1 %copy-start.6 = (bf16[512,128]{1,0:T(8,128)(2,1)S(1)}, bf16[512,128]{1,0:T(8,128)(2,1)}, u32[]{:S(2)}) copy-start(bf16[512,128]{1,0:T(8,128)(2,1)} %param.20) | copy-start | bytes 393220
  60.1 13.7 %copy-start.10 = (bf16[512,128]{1,0:T(8,128)(2,1)S(1)}, bf16[512,128]{1,0:T(8,128)(2,1)}, u32[]{:S(2)}) copy-start(bf16[512,128]{1,0:T(8,128)(2,1)} %copy-done.9) | copy-start | bytes 393220
  60.2 13.8 %copy-start.8 = (bf16[512,128]{1,0:T(8,128)(2,1)S(1)}, bf16[512,128]{1,0:T(8,128)(2,1)}, u32[]{:S(2)}) copy-start(bf16[512,128]{1,0:T(8,128)(2,1)} %copy-done.7) | copy-start | bytes 393220
  78.7 3.5 copy-start.1
  88.0 3.5 copy-start.1
  97.2 3.5 copy-start.1
  106.4 3.5 copy-start.1
  115.6 3.5 copy-start.1
  124.9 3.5 copy-start.1
  134.1 3.5 copy-start.1
  143.3 3.5 copy-start.1
  148.9 5.3 %copy-start.14 = (f32[512]{0:T(512)S(1)}, f32[512]{0:T(512)}, u32[]{:S(2)}) copy-start(f32[512]{0:T(512)} %fusion.25) | copy-start | bytes 6148
  149.7 13.5 %copy-start.5 = (bf16[128,2048]{1,0:T(8,128)(2,1)S(1)}, bf16[128,2048]{1,0:T(8,128)(2,1)}, u32[]{:S(2)}) copy-start(bf16[128,2048]{1,0:T(8,128)(2,1)} %param.21) | copy-start | bytes 1572868
  150.7 12.3 %all-to-all-start = ((bf16[4,128,512]{2,1,0:T(8,128)(2,1)}), bf16[4,128,512]{2,1,0:T(8,128)(2,1)S(1)}, u32[]{:S(2)}, u32[]{:S(2)}) async-start(bf16[4,128,512]{2,1,0:T(8,128)(2,1)} %all_to_all.20), calls=%async_computation | async-start | bytes 1048576 | tf_op jit(solution)/shard_map/all_to_all | solution.py:127
  163.3 4.8 %copy-start.12 = (f32[2048]{0:T(1024)S(1)}, f32[2048]{0:T(1024)}, u32[]{:S(2)}) copy-start(f32[2048]{0:T(1024)} %param.25) | copy-start | bytes 24580
  169.4 97.5 %copy-start.16 = (bf16[1,2048,256]{2,1,0:T(8,128)(2,1)S(1)}, bf16[1,2048,256]{2,1,0:T(8,128)(2,1)}, u32[]{:S(2)}) copy-start(bf16[1,2048,256]{2,1,0:T(8,128)(2,1)} %param.28) | copy-start | bytes 3145732
  278.3 3.8 copy-start.13
  278.3 4.0 %copy-start.4 = (bf16[2048,256]{1,0:T(8,128)(2,1)S(1)}, bf16[2048,256]{1,0:T(8,128)(2,1)}, u32[]{:S(2)}) copy-start(bf16[2048,256]{1,0:T(8,128)(2,1)} %param.31) | copy-start | bytes 3145732
  278.3 97.4 %all-to-all-start.2 = ((bf16[32,32,2048]{2,1,0:T(8,128)(2,1)}), bf16[32,32,2048]{2,1,0:T(8,128)(2,1)}, u32[]{:S(2)}, u32[]{:S(2)}) async-start(bf16[32,32,2048]{2,1,0:T(8,128)(2,1)} %convolution_convert_fusion), calls=%async_computation.2 | async-start | bytes 8388608 | tf_op jit(solution)/shard_map/all_to_all | solution.py:167
  387.8 3.9 copy-start.3
  (2 other events, 3.8 us)
Sparse Core Ops, SparseCore 0:
  12.8 43.6 all-gather.2
